TPU v7x, 128 devices: a whole 4x4x4 slice. The times are simulated.
128 devices in a mesh: fs: 16 (over z, y), tp: 8 (over x, core).
Axes of the slice: x: 4, y: 4, z: 4, core: 2. Of those that a mesh axis runs over, the one named last changes fastest.
Arguments:
- tokens: bfloat16 [12288, 2048], P('fs', 'tp'), may hold values from -40 to 40
- gain_one: float32 [2048], P('tp'), may hold values from 0.1 to 1.9
- w_gate: float32 [2048, 3072], P('fs', 'tp'), may hold values from -0.125 to 0.125
- w_up: float32 [2048, 3072], P('fs', 'tp'), may hold values from -0.125 to 0.125
- w_down: float32 [3072, 2048], P('tp', 'fs'), may hold values from -0.109375 to 0.109375
- scale_gate: float32 [3072], P('tp'), may hold values from 0.5 to 2
- scale_up: float32 [3072], P('tp'), may hold values from 0.5 to 2
- scale_down: float32 [2048], P('tp'), may hold values from 0.5 to 2
- gain_mix: float32 [2048], P('tp'), may hold values from 0.1 to 1.9
- w_query: float32 [2048, 2048], P('fs', 'tp'), may hold values from -0.125 to 0.125
- w_key: float32 [2048, 2048], P('fs', 'tp'), may hold values from -0.125 to 0.125
- w_value: float32 [2048, 2048], P('fs', 'tp'), may hold values from -0.125 to 0.125
- w_outgate: float32 [2048, 2048], P('fs', 'tp'), may hold values from -0.125 to 0.125
- scale_query: float32 [2048], P('tp'), may hold values from 0.5 to 2
- scale_key: float32 [2048], P('tp'), may hold values from 0.5 to 2
- scale_value: float32 [2048], P('tp'), may hold values from 0.5 to 2
- scale_outgate: float32 [2048], P('tp'), may hold values from 0.5 to 2
- ret_gain: float32 [2048], P('tp'), may hold values from 0.1 to 1.9
- decay_rate: float32 [8], P('tp'), may hold values from 0 to 2
- w_mix: float32 [2048, 2048], P('tp', 'fs'), may hold values from -0.125 to 0.125
- scale_mix: float32 [2048], P('tp'), may hold values from 0.5 to 2
- gain_two: float32 [2048], P('tp'), may hold values from 0.1 to 1.9
Outputs:
- layer_out: bfloat16 [12288, 2048], P('fs', 'tp')
All inputs are finite; a program needn't handle non-finite values.
Results may differ from a plain program's by a relative error of at most 0.022.
Values may be sent and summed in bfloat16 or wider, within the bound.
A program may use at most 128 MiB of HBM per device.

v0:
```python
import jax
import jax.numpy as jnp
from jax import lax
from jax.sharding import PartitionSpec as P

D = 2048
LEN = 256
BLK = 128
EPS = 1e-06
HEAD_EPS = 0.1


def from_everyone(shard, axis):
    copies = jnp.broadcast_to(shard, (lax.axis_size(axis), *shard.shape))
    return lax.all_to_all(copies, axis, split_axis=0, concat_axis=0, tiled=True)


def taken_together(shard, axis):
    return from_everyone(shard, axis).sum(axis=0)


def in_blocks(shard, dim, length):
    shape = shard.shape
    blocks = shard.reshape(*shape[:dim], length, shape[dim] // length, *shape[dim + 1 :])
    return jnp.moveaxis(blocks, dim, 0)


def sent_and_summed(shard, axis, dim):
    length = lax.axis_size(axis)
    blocks = lax.all_to_all(in_blocks(shard, dim, length), axis, 0, 0, tiled=True)
    return jnp.sum(blocks.astype(jnp.float32), axis=0)


def side_by_side(arrays, axis, dim, along):
    widths = [a.shape[along] for a in arrays]
    both = jnp.concatenate(arrays, axis=along)
    out = lax.all_gather(both, axis, axis=dim, tiled=True)
    return tuple(jnp.split(out, [sum(widths[:k]) for k in range(1, len(widths))], axis=along))


def laid_out(blocks, dim):
    blocks = jnp.moveaxis(blocks, 0, dim)
    shape = blocks.shape
    return blocks.reshape(*shape[:dim], shape[dim] * shape[dim + 1], *shape[dim + 2 :])


def gathered_copies(shard, axis, dim):
    return laid_out(from_everyone(shard, axis), dim)


def rotate_pairs(values):
    paired = values.reshape(values.shape[:-1] + (values.shape[-1] // 2, 2))
    return jnp.stack((-paired[..., 1], paired[..., 0]), axis=-1).reshape(values.shape)


def retain(query_rows, key_rows, value_rows, decay_rate, length, block):
    total_rows = query_rows.shape[0]
    heads = decay_rate.shape[0]
    head_size = query_rows.shape[1] // heads
    sequences = total_rows // length
    nblocks = length // block

    def split_heads(values):
        return values.astype(jnp.float32).reshape(sequences, length, heads, head_size)

    freq = 1.0 / 10000.0 ** jnp.linspace(0.0, 1.0, head_size // 2, dtype=jnp.float32)
    freq = jnp.repeat(freq, 2)
    angles = jnp.arange(length, dtype=jnp.float32)[:, None] * freq[None, :]
    sines = jnp.sin(angles)[None, :, None, :]
    cosines = jnp.cos(angles)[None, :, None, :]
    queries = split_heads(query_rows)
    queries = queries * cosines + rotate_pairs(queries) * sines
    keys_all = split_heads(key_rows) * head_size ** (-0.5)
    keys_all = keys_all * cosines + rotate_pairs(keys_all) * sines
    values_all = split_heads(value_rows)
    log_decay = -decay_rate
    offsets = jnp.arange(block, dtype=jnp.float32)
    distance = offsets[:, None] - offsets[None, :]
    inside = jnp.where(
        distance >= 0, jnp.exp(log_decay[:, None, None] * jnp.maximum(distance, 0.0)), 0.0
    )
    query_decay = jnp.exp(log_decay[None, :] * (offsets[:, None] + 1.0))
    key_decay = jnp.exp(log_decay[None, :] * (block - 1.0 - offsets[:, None]))
    block_decay = jnp.exp(log_decay * block)

    def to_blocks(values):
        return jnp.moveaxis(values.reshape(sequences, nblocks, block, heads, head_size), 1, 0)

    def advance(carried, pieces):
        query_blk, key_blk, value_blk = pieces
        scores = jnp.einsum("snhd,smhd->shnm", query_blk, key_blk) * inside
        within = jnp.einsum("shnm,smhe->snhe", scores, value_blk)
        across = jnp.einsum("snhd,shde->snhe", query_blk, carried) * query_decay[None, :, :, None]
        weighted = key_blk * key_decay[None, :, :, None]
        carried = carried * block_decay[None, :, None, None] + jnp.einsum(
            "smhd,smhe->shde", weighted, value_blk
        )
        return (carried, within + across)

    initial = jnp.zeros((sequences, heads, head_size, head_size), jnp.float32)
    _, results = lax.scan(
        advance, initial, (to_blocks(queries), to_blocks(keys_all), to_blocks(values_all))
    )
    results = jnp.moveaxis(results, 0, 1).reshape(sequences, length, heads, head_size)
    results = results * lax.rsqrt(jnp.mean(results * results, axis=-1, keepdims=True) + HEAD_EPS)
    return results.reshape(total_rows, heads * head_size)


def normed_rows(hidden_in, norm_gain):
    widened = hidden_in.astype(jnp.float32)
    totals = taken_together(jnp.sum(widened * widened, axis=1), "tp")
    scaled = widened * lax.rsqrt(totals / D + EPS)[:, None] * norm_gain
    return lax.all_gather(scaled.astype(jnp.bfloat16), "tp", axis=1, tiled=True)


def summed_share(partial_value):
    rounded = lax.optimization_barrier(partial_value.astype(jnp.bfloat16))
    return sent_and_summed(rounded.astype(jnp.float32).astype(jnp.bfloat16), "tp", 1)


def ffn_gathered(features, gate_low, up_low, down_low, scale_gate, scale_up):
    pieces = side_by_side((gate_low, up_low), "fs", 0, 1)
    gate_add = jnp.dot(features, pieces[0], preferred_element_type=jnp.float32)
    up_add = jnp.dot(features, pieces[1], preferred_element_type=jnp.float32)
    hidden = (jax.nn.silu(gate_add * scale_gate) * (up_add * scale_up)).astype(jnp.bfloat16)
    return jnp.dot(hidden, gathered_copies(down_low, "fs", 1), preferred_element_type=jnp.float32)


def per_device(
    tokens,
    gain_one,
    w_gate,
    w_up,
    w_down,
    scale_gate,
    scale_up,
    scale_down,
    gain_mix,
    w_query,
    w_key,
    w_value,
    w_outgate,
    scale_query,
    scale_key,
    scale_value,
    scale_outgate,
    ret_gain,
    decay_rate,
    w_mix,
    scale_mix,
    gain_two,
):
    norm_one, norm_mix, norm_two, down_cols, mix_cols = (
        gain_one,
        gain_mix,
        gain_two,
        scale_down,
        scale_mix,
    )
    gate_low = w_gate.astype(jnp.bfloat16)
    up_low = w_up.astype(jnp.bfloat16)
    down_low = w_down.astype(jnp.bfloat16)
    ffn_one = ffn_gathered(
        normed_rows(tokens, norm_one), gate_low, up_low, down_low, scale_gate, scale_up
    )
    first = (tokens.astype(jnp.float32) + 0.5 * summed_share(ffn_one) * down_cols).astype(
        jnp.bfloat16
    )
    features = normed_rows(first, norm_mix)
    pieces = side_by_side(
        (
            w_query.astype(jnp.bfloat16),
            w_key.astype(jnp.bfloat16),
            w_value.astype(jnp.bfloat16),
            w_outgate.astype(jnp.bfloat16),
        ),
        "fs",
        0,
        1,
    )
    query_pre, key_pre, value_pre, outgate_pre = tuple(
        (jnp.dot(features, piece, preferred_element_type=jnp.float32) for piece in pieces)
    )
    query_rows = (query_pre * scale_query).astype(jnp.bfloat16)
    key_rows = (key_pre * scale_key).astype(jnp.bfloat16)
    value_rows = (value_pre * scale_value).astype(jnp.bfloat16)
    outgate_rows = (outgate_pre * scale_outgate).astype(jnp.bfloat16)
    retained = retain(query_rows, key_rows, value_rows, decay_rate, LEN, BLK)
    mixed = (retained * ret_gain * jax.nn.silu(outgate_rows.astype(jnp.float32))).astype(
        jnp.bfloat16
    )
    mix_partial = jnp.dot(
        mixed,
        gathered_copies(w_mix.astype(jnp.bfloat16), "fs", 1),
        preferred_element_type=jnp.float32,
    )
    second = (first.astype(jnp.float32) + summed_share(mix_partial) * mix_cols).astype(jnp.bfloat16)
    ffn_two = ffn_gathered(
        normed_rows(second, norm_two), gate_low, up_low, down_low, scale_gate, scale_up
    )
    result = (second.astype(jnp.float32) + 0.5 * summed_share(ffn_two) * down_cols).astype(
        jnp.bfloat16
    )
    return result


def solution(mesh):
    return jax.shard_map(
        per_device,
        mesh=mesh,
        in_specs=(
            P("fs", "tp"),
            P("tp"),
            P("fs", "tp"),
            P("fs", "tp"),
            P("tp", "fs"),
            P("tp"),
            P("tp"),
            P("tp"),
            P("tp"),
            P("fs", "tp"),
            P("fs", "tp"),
            P("fs", "tp"),
            P("fs", "tp"),
            P("tp"),
            P("tp"),
            P("tp"),
            P("tp"),
            P("tp"),
            P("tp"),
            P("tp", "fs"),
            P("tp"),
            P("tp"),
        ),
        out_specs=P("fs", "tp"),
        check_vma=False,
    )
```

profile of v0, /device:TPU:1, one launch (start us, length us, event | category | flops | bytes accessed | tf_op | source)
XLA Modules:
  0.0 379.9 jit_solution(7782225091500418627)
XLA Ops:
  6.6 1.2 fusion.52
  7.9 10.3 %all_to_all.44 = f32[8,1,768]{2,1,0:T(1,128)S(1)} all-to-all(f32[8,1,768]{2,1,0:T(1,128)S(1)} %broadcast_in_dim.23), channel_id=1, replica_groups=mesh['fs'=16,'tp'=8] {'tp'}, dimensions={0} | all-to-all | bytes 49152 | tf_op jit(solution)/shard_map/all_to_all | solution.py:15
  18.2 1.9 fusion.54
  20.2 0.9 convert_element_type.111
  21.1 0.9 convert_element_type.112
  22.1 0.7 pad_maximum_fusion.3
  22.8 0.9 convert_element_type.120
  23.8 0.7 pad_maximum_fusion.2
  24.8 1.3 broadcast_in_dim.24
  26.1 7.8 %all-to-all-start.1 = ((bf16[16,384,128]{1,2,0:T(8,128)(2,1)}), bf16[16,384,128]{1,2,0:T(8,128)(2,1)S(1)}, u32[]{:S(2)}, u32[]{:S(2)}) async-start(bf16[16,384,128]{1,2,0:T(8,128)(2,1)} %broadcast_in_dim.24), calls=%async_computation.1 | async-start | bytes 3145728 | tf_op jit(solution)/shard_map/all_to_all | solution.py:15
  33.9 18.4 %all-gather.6.cloned.1.call-done = bf16[768,2048]{1,0:T(8,128)(2,1)} async-done(((bf16[768,256]{1,0:T(8,128)(2,1)}), bf16[768,2048]{1,0:T(8,128)(2,1)}) %all-gather.6.cloned.1.call-update) | async-done | bytes 3145744 | tf_op jit(solution)/shard_map/all_gather | solution.py:113
  52.3 50.1 %all-gather.8.cloned.1.call-done = bf16[2048,768]{1,0:T(8,128)(2,1)} async-done(((bf16[128,768]{1,0:T(8,128)(2,1)}), bf16[2048,768]{1,0:T(8,128)(2,1)}) %all-gather.8.cloned.1.call-update) | async-done | bytes 3145744 | tf_op jit(solution)/shard_map/all_gather | solution.py:37
  102.4 5.2 %convolution_multiply_fusion.4 = f32[768,384]{1,0:T(8,128)} fusion(bf16[768,2048]{1,0:T(8,128)(2,1)} %all-gather.6.cloned.1.call-done, bf16[2048,768]{1,0:T(8,128)(2,1)} %all-gather.8.cloned.1.call-done, f32[384]{0:T(512)S(1)} %copy-done.21), kind=kOutput, calls=%fused_computation.47 | convolution fusion | flops 1208254464 | bytes 5899776 | tf_op jit(solution)/shard_map/dot_general | solution.py:123
  107.6 1.1 copy-done.7
  108.8 6.7 %convolution_convert_fusion.2 = bf16[768,2048]{1,0:T(8,128)(2,1)S(1)} fusion(bf16[384,2048]{0,1:T(8,128)(2,1)} %bitcast.163, bf16[768,2048]{1,0:T(8,128)(2,1)} %all-gather.6.cloned.1.call-done, bf16[2048,768]{1,0:T(8,128)(2,1)} %all-gather.8.cloned.1.call-done, f32[768,384]{1,0:T(8,128)} %convolution_multiply_fusion.4, f32[384]{0:T(512)S(1)} %copy-done.22), kind=kOutput, calls=%fused_computation.38 | convolution fusion | flops 2419556352 | bytes 10618368 | tf_op jit(solution)/shard_map/dot_general | solution.py:126
  115.4 2.0 copy.141
  117.4 5.7 %all-to-all-start.2 = ((bf16[8,768,256]{2,1,0:T(8,128)(2,1)}), bf16[8,768,256]{2,1,0:T(8,128)(2,1)S(1)}, u32[]{:S(2)}, u32[]{:S(2)}) async-start(bf16[8,768,256]{2,1,0:T(8,128)(2,1)} %bitcast.116), calls=%async_computation.2 | async-start | bytes 6291456 | tf_op jit(solution)/shard_map/all_to_all | solution.py:30
  123.1 37.4 %all-to-all-done.2 = bf16[8,768,256]{2,1,0:T(8,128)(2,1)S(1)} async-done(((bf16[8,768,256]{2,1,0:T(8,128)(2,1)}), bf16[8,768,256]{2,1,0:T(8,128)(2,1)S(1)}, u32[]{:S(2)}, u32[]{:S(2)}) %all-to-all-start.2) | async-done | bytes 3145760 | tf_op jit(solution)/shard_map/all_to_all | solution.py:30
  160.5 0.4 convert_reduce_fusion.2
  161.2 8.0 %all_to_all.45 = f32[8,1,768]{2,1,0:T(1,128)S(1)} all-to-all(f32[8,1,768]{2,1,0:T(1,128)S(1)} %broadcast_in_dim.27), channel_id=1, replica_groups=mesh['fs'=16,'tp'=8] {'tp'}, dimensions={0} | all-to-all | bytes 49152 | tf_op jit(solution)/shard_map/all_to_all | solution.py:15
  169.3 0.9 fusion.58
  170.2 0.9 convert_element_type.132
  171.3 1.1 broadcast_in_dim.31
  172.3 4.3 %all-to-all-start.4 = ((bf16[16,256,128]{1,2,0:T(8,128)(2,1)}), bf16[16,256,128]{1,2,0:T(8,128)(2,1)}, u32[]{:S(2)}, u32[]{:S(2)}) async-start(bf16[16,256,128]{1,2,0:T(8,128)(2,1)} %broadcast_in_dim.31), calls=%async_computation.4 | async-start | bytes 2097152 | tf_op jit(solution)/shard_map/all_to_all | solution.py:15
  178.0 8.5 %multiply_cosine_fusion = (f32[2,128,256]{1,0,2:T(2,128)}, f32[2,128,256]{1,0,2:T(2,128)}, f32[2,128,256]{1,0,2:T(2,128)}) fusion(f32[2,128]{1,0:T(2,128)S(1)} %multiply_add_fusion, f32[256]{0:T(256)S(1)} %mul.470), kind=kLoop, calls=%fused_computation.107 | loop fusion | flops 327680 | bytes 788480 | tf_op jit(solution)/shard_map/cos | solution.py:70
  186.5 12.2 %all-gather.10.cloned.1.call-done = bf16[768,2048]{1,0:T(8,128)(2,1)} async-done(((bf16[768,256]{1,0:T(8,128)(2,1)}), bf16[768,2048]{1,0:T(8,128)(2,1)}) %all-gather.10.cloned.1.call-update) | async-done | bytes 3145744 | tf_op jit(solution)/shard_map/all_gather | solution.py:113
  198.7 4.1 %broadcast_multiply_fusion = (f32[768,256]{1,0:T(8,128)S(1)}, f32[768,256]{1,0:T(8,128)}) fusion(f32[256]{0:T(256)S(1)} %copy-done.24, bf16[768,2048]{1,0:T(8,128)(2,1)} %all-gather.10.cloned.1.call-done, bf16[2048,1024]{1,0:T(8,128)(2,1)} %all-gather.12.cloned.1.call-done), kind=kOutput, calls=%fused_computation.106 | convolution fusion | flops 806092800 | bytes 5768192 | tf_op jit(solution)/shard_map/dot_general | solution.py:182
  202.8 0.3 copy.108
  203.1 0.4 mul.479
  204.0 1.7 copy.109
  205.7 2.2 fusion.41
  207.9 0.3 copy.112
  208.2 0.4 reshape_reshape.8
  209.1 1.7 copy.113
  210.8 1.2 copy.107
  212.0 1.2 copy.111
  213.3 3.3 fusion.39
  216.7 1.9 add_bitcast_fusion
  218.5 8.8 %while.15 = (s32[]{:T(128)}, f32[3,1,256,256]{3,2,0,1:T(8,128)S(1)}, f32[2,3,128,1,256]{2,4,1,3,0:T(8,128)}, f32[1]{0:T(128)}, f32[2,3,128,1,256]{2,0,3,4,1:T(2,...) while((s32[]{:T(128)}, ...), condition=%wide.region_6.7_spmd.clone.clone.clone, body=%wide.region_5.6_spmd.clone.clone.clone.sunk | while | flops 152257024 | bytes 7998088 | solution.py:101
  218.5 2.0 constant_dynamic-slice_fusion.3
  220.6 0.4 convolution_bitcast_fusion.4
  221.0 1.1 fusion.108
  222.1 0.3 copy.144
  222.4 0.4 fusion.107
  222.8 1.9 constant_dynamic-slice_fusion.3
  224.8 0.4 convolution_bitcast_fusion.4
  225.3 1.1 fusion.108
  226.4 0.3 copy.144
  226.7 0.4 fusion.107
  227.3 1.4 copy.116
  228.8 1.2 multiply_reduce_fusion
  230.0 3.2 fusion.66
  233.3 2.2 convolution_convert_fusion.1
  235.7 41.4 %all_to_all.46 = bf16[8,768,256]{2,1,0:T(8,128)(2,1)S(1)} all-to-all(bf16[8,768,256]{2,1,0:T(8,128)(2,1)S(1)} %bitcast.155), channel_id=1, replica_groups=mesh['fs'=16,'tp'=8] {'tp'}, dimensions={0} | all-to-all | bytes 6291456 | tf_op jit(solution)/shard_map/all_to_all | solution.py:30
  277.1 0.4 convert_reduce_fusion.1
  277.6 0.5 copy-done.2
  278.4 8.1 %all_to_all.47 = f32[8,1,768]{2,1,0:T(1,128)S(1)} all-to-all(f32[8,1,768]{2,1,0:T(1,128)S(1)} %broadcast_in_dim.32), channel_id=1, replica_groups=mesh['fs'=16,'tp'=8] {'tp'}, dimensions={0} | all-to-all | bytes 49152 | tf_op jit(solution)/shard_map/all_to_all | solution.py:15
  286.5 0.9 fusion.62
  287.5 31.1 %all-gather.14.cloned.1.call-done = bf16[768,2048]{1,0:T(8,128)(2,1)} async-done(((bf16[768,256]{1,0:T(8,128)(2,1)}), bf16[768,2048]{1,0:T(8,128)(2,1)}) %all-gather.14.cloned.1.call-update) | async-done | bytes 3145744 | tf_op jit(solution)/shard_map/all_gather | solution.py:113
  318.6 5.3 %convolution_multiply_fusion.2 = f32[768,384]{1,0:T(8,128)} fusion(bf16[768,2048]{1,0:T(8,128)(2,1)} %all-gather.14.cloned.1.call-done, bf16[2048,768]{1,0:T(8,128)(2,1)} %all-gather.8.cloned.1.call-done, f32[384]{0:T(512)S(1)} %copy-done.21), kind=kOutput, calls=%fused_computation.44 | convolution fusion | flops 1208254464 | bytes 5899776 | tf_op jit(solution)/shard_map/dot_general | solution.py:123
  323.8 6.6 %convolution_convert_fusion = bf16[768,2048]{1,0:T(8,128)(2,1)S(1)} fusion(bf16[384,2048]{0,1:T(8,128)(2,1)} %bitcast.164, bf16[768,2048]{1,0:T(8,128)(2,1)} %all-gather.14.cloned.1.call-done, bf16[2048,768]{1,0:T(8,128)(2,1)} %all-gather.8.cloned.1.call-done, f32[768,384]{1,0:T(8,128)} %convolution_multiply_fusion.2, f32[384]{0:T(512)S(1)} %copy-done.23), kind=kOutput, calls=%fused_computation.36 | convolution fusion | flops 2419556352 | bytes 10618368 | tf_op jit(solution)/shard_map/dot_general | solution.py:126
  330.7 41.4 %all_to_all.48 = bf16[8,768,256]{2,1,0:T(8,128)(2,1)S(1)} all-to-all(bf16[8,768,256]{2,1,0:T(8,128)(2,1)S(1)} %bitcast.156), channel_id=1, replica_groups=mesh['fs'=16,'tp'=8] {'tp'}, dimensions={0} | all-to-all | bytes 6291456 | tf_op jit(solution)/shard_map/all_to_all | solution.py:30
  372.1 0.4 convert_reduce_fusion
  372.5 0.9 fusion.63
  (108 shorter events, 3.2 us)
Async XLA Ops:
  6.5 17.2 %copy-start.13 = (f32[128,256]{1,0:T(8,128)S(1)}, f32[128,256]{1,0:T(8,128)}, u32[]{:S(2)}) copy-start(f32[128,256]{1,0:T(8,128)} %param.34) | copy-start | bytes 393220
  6.5 17.2 %copy-start.14 = (f32[128,256]{1,0:T(8,128)S(1)}, f32[128,256]{1,0:T(8,128)}, u32[]{:S(2)}) copy-start(f32[128,256]{1,0:T(8,128)} %param.35) | copy-start | bytes 393220
  6.5 17.3 %copy-start.15 = (f32[128,256]{1,0:T(8,128)S(1)}, f32[128,256]{1,0:T(8,128)}, u32[]{:S(2)}) copy-start(f32[128,256]{1,0:T(8,128)} %param.36) | copy-start | bytes 393220
  6.5 18.1 %copy-start.12 = (f32[384,128]{1,0:T(8,128)S(1)}, f32[384,128]{1,0:T(8,128)}, u32[]{:S(2)}) copy-start(f32[384,128]{1,0:T(8,128)} %param.28) | copy-start | bytes 589828
  6.5 45.8 %all-gather.6.cloned.1.call-start = ((), (), s32[]{:S(2)}) async-start(), calls=%async_computation.8 | async-start | bytes 3538944 | tf_op jit(solution)/shard_map/all_gather | solution.py:113
  20.1 82.3 %all-gather.8.cloned.1.call-start = ((), (), s32[]{:S(2)}) async-start(), calls=%async_computation.9 | async-start | bytes 3342336 | tf_op jit(solution)/shard_map/all_gather | solution.py:37
  22.8 163.7 %all-gather.12.cloned.1.call-start = ((), (), s32[]{:S(2)}) async-start(), calls=%async_computation.11 | async-start | bytes 4456448 | tf_op jit(solution)/shard_map/all_gather | solution.py:37
  23.8 78.6 %copy-start.21 = (f32[384]{0:T(512)S(1)}, f32[384]{0:T(512)}, u32[]{:S(2)}) copy-start(f32[384]{0:T(512)} %param.29) | copy-start | bytes 4612
  26.1 81.5 %all-to-all-start.1 = ((bf16[16,384,128]{1,2,0:T(8,128)(2,1)}), bf16[16,384,128]{1,2,0:T(8,128)(2,1)S(1)}, u32[]{:S(2)}, u32[]{:S(2)}) async-start(bf16[16,384,128]{1,2,0:T(8,128)(2,1)} %broadcast_in_dim.24), calls=%async_computation.1 | async-start | bytes 3145728 | tf_op jit(solution)/shard_map/all_to_all | solution.py:15
  33.9 74.9 %copy-start.22 = (f32[384]{0:T(512)S(1)}, f32[384]{0:T(512)}, u32[]{:S(2)}) copy-start(f32[384]{0:T(512)} %param.30) | copy-start | bytes 4612
  107.6 1.1 copy-start.7
  117.4 5.7 %copy-start.18 = (f32[256]{0:T(256)S(1)}, f32[256]{0:T(256)}, u32[]{:S(2)}) copy-start(f32[256]{0:T(256)} %param.31) | copy-start | bytes 3076
  117.4 43.1 %all-to-all-start.2 = ((bf16[8,768,256]{2,1,0:T(8,128)(2,1)}), bf16[8,768,256]{2,1,0:T(8,128)(2,1)S(1)}, u32[]{:S(2)}, u32[]{:S(2)}) async-start(bf16[8,768,256]{2,1,0:T(8,128)(2,1)} %bitcast.116), calls=%async_computation.2 | async-start | bytes 6291456 | tf_op jit(solution)/shard_map/all_to_all | solution.py:30
  123.1 37.9 %copy-start = (bf16[768,256]{1,0:T(8,128)(2,1)S(1)}, bf16[768,256]{1,0:T(8,128)(2,1)}, u32[]{:S(2)}) copy-start(bf16[768,256]{1,0:T(8,128)(2,1)} %param.24) | copy-start | bytes 1179652
  123.1 46.2 %copy-start.16 = (f32[256]{0:T(256)S(1)}, f32[256]{0:T(256)}, u32[]{:S(2)}) copy-start(f32[256]{0:T(256)} %param.32) | copy-start | bytes 3076
  123.1 75.6 %all-gather.10.cloned.1.call-start = ((), (), s32[]{:S(2)}) async-start(), calls=%async_computation.10 | async-start | bytes 3538944 | tf_op jit(solution)/shard_map/all_gather | solution.py:113
  161.2 15.5 %copy-start.1 = (bf16[768,256]{1,0:T(8,128)(2,1)}, bf16[768,256]{1,0:T(8,128)(2,1)S(1)}, u32[]{:S(2)}) copy-start(bf16[768,256]{1,0:T(8,128)(2,1)S(1)} %get-tuple-element.210) | copy-start | bytes 1179652
  161.2 37.5 %copy-start.24 = (f32[256]{0:T(256)S(1)}, f32[256]{0:T(256)}, u32[]{:S(2)}) copy-start(f32[256]{0:T(256)} %param.38) | copy-start | bytes 3076
  172.3 60.9 %all-to-all-start.4 = ((bf16[16,256,128]{1,2,0:T(8,128)(2,1)}), bf16[16,256,128]{1,2,0:T(8,128)(2,1)}, u32[]{:S(2)}, u32[]{:S(2)}) async-start(bf16[16,256,128]{1,2,0:T(8,128)(2,1)} %broadcast_in_dim.31), calls=%async_computation.4 | async-start | bytes 2097152 | tf_op jit(solution)/shard_map/all_to_all | solution.py:15
  176.7 141.9 %all-gather.14.cloned.1.call-start = ((), (), s32[]{:S(2)}) async-start(), calls=%async_computation.12 | async-start | bytes 3538944 | tf_op jit(solution)/shard_map/all_gather | solution.py:113
  203.5 2.2 copy-start.20
  203.5 2.2 copy-start.25
  208.6 2.2 copy-start.11
  208.9 4.3 %copy-start.26 = (f32[256]{0:T(256)S(1)}, f32[256]{0:T(256)}, u32[]{:S(2)}) copy-start(f32[256]{0:T(256)} %param.39) | copy-start | bytes 3076
  213.2 3.4 copy-start.3
  213.2 3.4 copy-start.4
  213.2 3.4 copy-start.5
  213.2 3.4 copy-start.6
  213.2 3.4 copy-start.8
  213.2 3.4 copy-start.9
  213.2 3.4 copy-start.10
  218.5 11.5 %copy-start.27 = (f32[256]{0:T(256)S(1)}, f32[256]{0:T(256)}, u32[]{:S(2)}) copy-start(f32[256]{0:T(256)} %param.40) | copy-start | bytes 3076
  218.5 11.5 %copy-start.28 = (f32[256]{0:T(256)S(1)}, f32[256]{0:T(256)}, u32[]{:S(2)}) copy-start(f32[256]{0:T(256)} %param.41) | copy-start | bytes 3076
  277.1 1.0 copy-start.2
  277.1 1.0 copy-start.19
  277.1 9.4 %copy-start.17 = (f32[256]{0:T(256)S(1)}, f32[256]{0:T(256)}, u32[]{:S(2)}) copy-start(f32[256]{0:T(256)} %param.45) | copy-start | bytes 3076
  287.4 36.4 %copy-start.23 = (f32[384]{0:T(512)S(1)}, f32[384]{0:T(512)}, u32[]{:S(2)}) copy-start(f32[384]{0:T(512)} %param.30) | copy-start | bytes 4612
Sparse Core Ops, SparseCore 0:
  20.2 32.0 all-gather.5
  54.5 47.8 all-gather.7
  104.5 50.5 all-gather.11
  170.3 28.3 all-gather.9
  287.6 30.9 all-gather.13
where the time goes:
time: 381 us; the launch traced here: 380 us
  waiting for transfers between devices  149 us (39%)
  blocking collectives  109 us (29%)
  matrix products  42.7 us (11%)
  other arithmetic  25.7 us (7%)
  local copies, waits for them, and re-layouts  20.2 us (5%)
  starting transfers between devices  18.2 us (5%)
  between operations  14.5 us (4%)
    all_to_all x2, blocking collectives, sent_and_summed(): lax.all_to_all(in_blocks(shard, dim, length), axis, 0, 0, tiled=True)  82.8 us
    all_gather x3, waiting for transfers between devices, normed_rows(): return lax.all_gather(scaled.astype(jnp.bfloat16), 'tp', axis=1, tiled=True)  61.7 us
    all_gather x2, waiting for transfers between devices, side_by_side(): out = lax.all_gather(both, axis, axis=dim, tiled=True)  50.1 us
    all_to_all x1, waiting for transfers between devices, sent_and_summed(): lax.all_to_all(in_blocks(shard, dim, length), axis, 0, 0, tiled=True)  37.4 us
    all_to_all x3, blocking collectives, from_everyone(): return lax.all_to_all(copies, axis, split_axis=0, concat_axis=0, tiled=True)  26.4 us
    dot_general x2, matrix products, ffn_gathered(): jnp.dot(hidden, gathered_copies(down_low, 'fs', 1), preferred_element_typ...  13.3 us
    dot_general x4, matrix products, per_device(): jnp.dot(features, piece, preferred_element_type=jnp.float32)  12.8 us
    all_to_all x2, starting transfers between devices, from_everyone(): return lax.all_to_all(copies, axis, split_axis=0, concat_axis=0, tiled=True)  12.1 us
  transfers between devices with their start and end apart: 8, of which 5 were waited for; matrix products, arithmetic and copies ran while one was open for 17% of the time, Pallas kernels for 0%

commit v1 on v0

--- a/solution.py
+++ b/solution.py
@@ -8,6 +8,11 @@
 BLK = 128
 EPS = 1e-06
 HEAD_EPS = 0.1
+
+
+def gather_from_all(x, axis, dim):
+    copies = jnp.concatenate([x] * lax.axis_size(axis), axis=dim)
+    return lax.all_to_all(copies, axis, dim, dim, tiled=True)
 
 
 def from_everyone(shard, axis):
@@ -110,7 +115,7 @@
     widened = hidden_in.astype(jnp.float32)
     totals = taken_together(jnp.sum(widened * widened, axis=1), "tp")
     scaled = widened * lax.rsqrt(totals / D + EPS)[:, None] * norm_gain
-    return lax.all_gather(scaled.astype(jnp.bfloat16), "tp", axis=1, tiled=True)
+    return gather_from_all(scaled.astype(jnp.bfloat16), "tp", 1)
 
 
 def summed_share(partial_value):

time: 381 us -> 468 us (1.23)
  local copies, waits for them, and re-layouts: 20.2 us -> 62.8 us
  waiting for transfers between devices: 149 us -> 117 us
  blocking collectives: 109 us -> 140 us
  other arithmetic: 25.7 us -> 49.2 us
  starting transfers between devices: 18.2 us -> 36 us
    all_to_all x0 -> x2, waiting for transfers between devices: none -> 65.3 us  [gather_from_all(): return lax.all_to_all(copies, axis, dim, dim, tiled=True)]
    all_gather x3 -> x0, waiting for transfers between devices: 61.7 us -> none  [normed_rows(): return lax.all_gather(scaled.astype(jnp.bfloat16), 'tp', axis=1, tiled=True)]
    all_gather x2, waiting for transfers between devices: 50.1 us -> 0.01 us  [side_by_side(): out = lax.all_gather(both, axis, axis=dim, tiled=True)]
    all_to_all x0 -> x1, blocking collectives: none -> 42.6 us  [gather_from_all(): return lax.all_to_all(copies, axis, dim, dim, tiled=True)]
    all_to_all x0 -> x6, local copies, waits for them, and re-layouts: none -> 26.3 us  [gather_from_all(): return lax.all_to_all(copies, axis, dim, dim, tiled=True)]
    unnamed x1 -> x22, other arithmetic: 0.01 us -> 22.8 us
    all_to_all x2 -> x3, waiting for transfers between devices: 0.01 us -> 15.4 us  [from_everyone(): return lax.all_to_all(copies, axis, split_axis=0, concat_axis=0, tiled=True)]
    concatenate x0 -> x3, local copies, waits for them, and re-layouts: none -> 12.5 us  [gather_from_all(): copies = jnp.concatenate([x] * lax.axis_size(axis), axis=dim)]
  transfers between devices with their start and end apart: 8 -> 8, of which waited for: 5 -> 5; matrix products, arithmetic and copies ran while one was open for 17% -> 22% of each run, Pallas kernels for 0% -> 0%
where the time goes in v1:
time: 468 us; the launch traced here: 466 us
  blocking collectives  140 us (30%)
  waiting for transfers between devices  117 us (25%)
  local copies, waits for them, and re-layouts  62.8 us (13%)
  other arithmetic  49.2 us (11%)
  matrix products  45 us (10%)
  starting transfers between devices  36 us (8%)
  between operations  14.7 us (3%)
    all_to_all x2, blocking collectives, sent_and_summed(): lax.all_to_all(in_blocks(shard, dim, length), axis, 0, 0, tiled=True)  81.7 us
    all_to_all x2, waiting for transfers between devices, gather_from_all(): return lax.all_to_all(copies, axis, dim, dim, tiled=True)  65.3 us
    all_to_all x1, blocking collectives, gather_from_all(): return lax.all_to_all(copies, axis, dim, dim, tiled=True)  42.6 us
    all_to_all x1, waiting for transfers between devices, sent_and_summed(): lax.all_to_all(in_blocks(shard, dim, length), axis, 0, 0, tiled=True)  36.7 us
    all_to_all x6, local copies, waits for them, and re-layouts, gather_from_all(): return lax.all_to_all(copies, axis, dim, dim, tiled=True)  26.3 us
    unnamed x22, other arithmetic  22.8 us
    all_to_all x3, starting transfers between devices, from_everyone(): return lax.all_to_all(copies, axis, split_axis=0, concat_axis=0, tiled=True)  18.1 us
    all_to_all x2, blocking collectives, from_everyone(): return lax.all_to_all(copies, axis, split_axis=0, concat_axis=0, tiled=True)  16.2 us
  transfers between devices with their start and end apart: 8, of which 5 were waited for; matrix products, arithmetic and copies ran while one was open for 22% of the time, Pallas kernels for 0%

profile of v1, /device:TPU:1, one launch (start us, length us, event | category | flops | bytes accessed | tf_op | source)
XLA Modules:
  0.0 465.8 jit_solution(654511738879370604)
XLA Ops:
  6.5 1.2 fusion.52
  8.4 5.8 %all-to-all-start = ((f32[8,1,768]{2,1,0:T(1,128)}), f32[8,1,768]{2,1,0:T(1,128)S(1)}, u32[]{:S(2)}, u32[]{:S(2)}) async-start(f32[8,1,768]{2,1,0:T(1,128)} %broadcast_in_dim.23), calls=%async_computation | async-start | bytes 49152 | tf_op jit(solution)/shard_map/all_to_all | solution.py:20
  16.8 2.1 all-to-all-done
  18.9 2.0 constant_dynamic-update-slice_fusion.7
  20.9 2.0 constant_dynamic-update-slice_fusion.6
  22.9 1.0 constant_dynamic-update-slice_fusion.5
  25.9 1.0 constant_dynamic-update-slice_fusion.2
  28.9 4.7 %copy.149 = bf16[768,2048]{0,1:T(8,128)(2,1)} copy(bf16[768,2048]{1,0:T(8,128)(2,1)} %constant_dynamic-update-slice_fusion) | data formatting | bytes 6291456 | tf_op jit(solution)/shard_map/concatenate | solution.py:14
  33.6 4.7 %copy.150 = bf16[768,8,256]{2,0,1:T(8,128)(2,1)} copy(bf16[768,8,256]{0,2,1:T(8,128)(2,1)} %bitcast.162) | data formatting | bytes 6291456 | tf_op jit(solution)/shard_map/all_to_all | solution.py:15
  38.3 5.2 %all-to-all-start.1 = ((bf16[768,8,256]{2,0,1:T(8,128)(2,1)}), bf16[768,8,256]{2,0,1:T(8,128)(2,1)}, u32[]{:S(2)}, u32[]{:S(2)}) async-start(bf16[768,8,256]{2,0,1:T(8,128)(2,1)} %copy.150), calls=%async_computation.1 | async-start | bytes 6291456 | tf_op jit(solution)/shard_map/all_to_all | solution.py:15
  43.6 37.4 %all-to-all-done.1 = bf16[768,8,256]{2,0,1:T(8,128)(2,1)} async-done(((bf16[768,8,256]{2,0,1:T(8,128)(2,1)}), bf16[768,8,256]{2,0,1:T(8,128)(2,1)}, u32[]{:S(2)}, u32[]{:S(2)}) %all-to-all-start.1) | async-done | bytes 3145760 | tf_op jit(solution)/shard_map/all_to_all | solution.py:15
  81.0 1.3 broadcast_in_dim.24
  82.3 7.8 %all-to-all-start.2 = ((bf16[16,384,128]{1,2,0:T(8,128)(2,1)}), bf16[16,384,128]{1,2,0:T(8,128)(2,1)S(1)}, u32[]{:S(2)}, u32[]{:S(2)}) async-start(bf16[16,384,128]{1,2,0:T(8,128)(2,1)} %broadcast_in_dim.24), calls=%async_computation.2 | async-start | bytes 3145728 | tf_op jit(solution)/shard_map/all_to_all | solution.py:20
  90.1 4.7 %copy.151 = bf16[768,8,256]{0,2,1:T(8,128)(2,1)} copy(bf16[768,8,256]{2,0,1:T(8,128)(2,1)} %all-to-all-done.1) | data formatting | bytes 6291456 | tf_op jit(solution)/shard_map/all_to_all | solution.py:15
  94.8 4.2 convolution_multiply_fusion.4
  99.0 13.3 %all-to-all-done.2 = bf16[16,384,128]{1,2,0:T(8,128)(2,1)S(1)} async-done(((bf16[16,384,128]{1,2,0:T(8,128)(2,1)}), bf16[16,384,128]{1,2,0:T(8,128)(2,1)S(1)}, u32[]{:S(2)}, u32[]{:S(2)}) %all-to-all-start.2) | async-done | bytes 1572896 | tf_op jit(solution)/shard_map/all_to_all | solution.py:20
  112.3 8.1 %convolution_convert_fusion.2 = bf16[768,2048]{1,0:T(8,128)(2,1)} fusion(bf16[384,2048]{0,1:T(8,128)(2,1)S(1)} %bitcast.181, bf16[768,2048]{0,1:T(8,128)(2,1)} %bitcast.172, bf16[2048,768]{1,0:T(8,128)(2,1)} %all-gather.3.cloned.1.call-done, f32[768,384]{1,0:T(8,128)S(1)} %convolution_multiply_fusion.4, f32[384]{0:T(512)S(1)} %copy-done.26), kind=kOutput, calls=%fused_computation.38 | convolution fusion | flops 2419556352 | bytes 10618368 | tf_op jit(solution)/shard_map/dot_general | solution.py:131
  120.4 3.8 copy.195
  124.3 7.6 %all-to-all-start.3 = ((bf16[8,768,256]{2,1,0:T(8,128)(2,1)}), bf16[8,768,256]{2,1,0:T(8,128)(2,1)}, u32[]{:S(2)}, u32[]{:S(2)}) async-start(bf16[8,768,256]{2,1,0:T(8,128)(2,1)} %bitcast.160), calls=%async_computation.3 | async-start | bytes 6291456 | tf_op jit(solution)/shard_map/all_to_all | solution.py:35
  132.8 36.7 %all-to-all-done.3 = bf16[8,768,256]{2,1,0:T(8,128)(2,1)} async-done(((bf16[8,768,256]{2,1,0:T(8,128)(2,1)}), bf16[8,768,256]{2,1,0:T(8,128)(2,1)}, u32[]{:S(2)}, u32[]{:S(2)}) %all-to-all-start.3) | async-done | bytes 3145760 | tf_op jit(solution)/shard_map/all_to_all | solution.py:35
  169.5 2.4 convert_reduce_fusion.2
  172.2 8.1 %all_to_all.80 = f32[8,1,768]{2,1,0:T(1,128)S(1)} all-to-all(f32[8,1,768]{2,1,0:T(1,128)S(1)} %broadcast_in_dim.27), channel_id=1, replica_groups=mesh['fs'=16,'tp'=8] {'tp'}, dimensions={0} | all-to-all | bytes 49152 | tf_op jit(solution)/shard_map/all_to_all | solution.py:20
  181.3 1.0 constant_dynamic-update-slice_fusion.14
  182.3 1.0 constant_dynamic-update-slice_fusion.13
  185.3 1.0 constant_dynamic-update-slice_fusion.10
  188.3 3.2 copy.155
  191.4 2.9 copy.156
  194.3 5.1 %all-to-all-start.5 = ((bf16[768,8,256]{2,0,1:T(8,128)(2,1)}), bf16[768,8,256]{2,0,1:T(8,128)(2,1)}, u32[]{:S(2)}, u32[]{:S(2)}) async-start(bf16[768,8,256]{2,0,1:T(8,128)(2,1)} %copy.156), calls=%async_computation.5 | async-start | bytes 6291456 | tf_op jit(solution)/shard_map/all_to_all | solution.py:15
  200.6 8.6 %multiply_cosine_fusion = (f32[2,128,256]{1,0,2:T(2,128)}, f32[2,128,256]{1,0,2:T(2,128)}, f32[2,128,256]{1,0,2:T(2,128)}) fusion(f32[2,128]{1,0:T(2,128)S(1)} %multiply_add_fusion, f32[256]{0:T(256)S(1)} %mul.470), kind=kLoop, calls=%fused_computation.107 | loop fusion | flops 327680 | bytes 788480 | tf_op jit(solution)/shard_map/cos | solution.py:75
  209.2 27.8 %all-to-all-done.5 = bf16[768,8,256]{2,0,1:T(8,128)(2,1)} async-done(((bf16[768,8,256]{2,0,1:T(8,128)(2,1)}), bf16[768,8,256]{2,0,1:T(8,128)(2,1)}, u32[]{:S(2)}, u32[]{:S(2)}) %all-to-all-start.5) | async-done | bytes 3145760 | tf_op jit(solution)/shard_map/all_to_all | solution.py:15
  237.0 1.1 broadcast_in_dim.31
  238.1 4.5 all-to-all-start.6
  242.6 4.7 %copy.157 = bf16[768,8,256]{0,2,1:T(8,128)(2,1)} copy(bf16[768,8,256]{2,0,1:T(8,128)(2,1)} %all-to-all-done.5) | data formatting | bytes 6291456 | tf_op jit(solution)/shard_map/all_to_all | solution.py:15
  247.3 4.1 broadcast_multiply_fusion
  252.6 1.7 copy.160
  254.4 2.2 fusion.41
  258.7 1.7 copy.164
  260.4 1.2 copy.158
  261.6 1.2 copy.162
  262.8 3.3 fusion.39
  266.3 1.8 add_bitcast_fusion
  268.1 11.7 %while.15 = (s32[]{:T(128)}, f32[3,1,256,256]{3,2,0,1:T(8,128)S(1)}, f32[2,3,128,1,256]{2,4,1,3,0:T(8,128)}, f32[1]{0:T(128)}, f32[2,3,128,1,256]{2,0,3,4,1:T(2,...) while((s32[]{:T(128)}, ...), condition=%wide.region_6.7_spmd.clone.clone.clone, body=%wide.region_5.6_spmd.clone.clone.clone.sunk | while | flops 152257024 | bytes 7998088 | solution.py:106
  268.1 1.9 constant_dynamic-slice_fusion.3
  270.8 1.2 convolution_bitcast_fusion.4
  272.0 1.1 fusion.108
  273.9 1.9 constant_dynamic-slice_fusion.3
  276.5 1.2 convolution_bitcast_fusion.4
  277.8 1.1 fusion.108
  279.8 1.4 copy.167
  281.2 1.2 multiply_reduce_fusion
  282.5 3.4 fusion.66
  285.9 2.2 convolution_convert_fusion.1
  288.3 40.8 %all_to_all.81 = bf16[8,768,256]{2,1,0:T(8,128)(2,1)S(1)} all-to-all(bf16[8,768,256]{2,1,0:T(8,128)(2,1)S(1)} %bitcast.164), channel_id=1, replica_groups=mesh['fs'=16,'tp'=8] {'tp'}, dimensions={0} | all-to-all | bytes 6291456 | tf_op jit(solution)/shard_map/all_to_all | solution.py:35
  330.1 8.1 %all_to_all.82 = f32[8,1,768]{2,1,0:T(1,128)S(1)} all-to-all(f32[8,1,768]{2,1,0:T(1,128)S(1)} %broadcast_in_dim.32), channel_id=1, replica_groups=mesh['fs'=16,'tp'=8] {'tp'}, dimensions={0} | all-to-all | bytes 49152 | tf_op jit(solution)/shard_map/all_to_all | solution.py:20
  340.2 1.0 constant_dynamic-update-slice_fusion.21
  343.2 1.0 constant_dynamic-update-slice_fusion.18
  346.2 4.7 %copy.172 = bf16[768,2048]{0,1:T(8,128)(2,1)} copy(bf16[768,2048]{1,0:T(8,128)(2,1)} %constant_dynamic-update-slice_fusion.16) | data formatting | bytes 6291456 | tf_op jit(solution)/shard_map/concatenate | solution.py:14
  350.8 4.7 %copy.173 = bf16[768,8,256]{2,0,1:T(8,128)(2,1)} copy(bf16[768,8,256]{0,2,1:T(8,128)(2,1)} %bitcast.165) | data formatting | bytes 6291456 | tf_op jit(solution)/shard_map/all_to_all | solution.py:15
  355.5 42.6 %all_to_all.83 = bf16[768,8,256]{2,0,1:T(8,128)(2,1)} all-to-all(bf16[768,8,256]{2,0,1:T(8,128)(2,1)} %copy.173), channel_id=1, replica_groups=mesh['fs'=16,'tp'=8] {'tp'}, dimensions={1} | all-to-all | bytes 6291456 | tf_op jit(solution)/shard_map/all_to_all | solution.py:15
  398.1 4.7 %copy.174 = bf16[768,8,256]{0,2,1:T(8,128)(2,1)} copy(bf16[768,8,256]{2,0,1:T(8,128)(2,1)} %all_to_all.83) | data formatting | bytes 6291456 | tf_op jit(solution)/shard_map/all_to_all | solution.py:15
  402.8 4.3 convolution_multiply_fusion.2
  407.0 7.6 %convolution_convert_fusion = bf16[768,2048]{1,0:T(8,128)(2,1)} fusion(bf16[384,2048]{0,1:T(8,128)(2,1)S(1)} %bitcast.182, bf16[768,2048]{0,1:T(8,128)(2,1)} %bitcast.174, bf16[2048,768]{1,0:T(8,128)(2,1)} %all-gather.3.cloned.1.call-done, f32[768,384]{1,0:T(8,128)S(1)} %convolution_multiply_fusion.2, f32[384]{0:T(512)S(1)} %copy-done.26), kind=kOutput, calls=%fused_computation.36 | convolution fusion | flops 2419556352 | bytes 10618368 | tf_op jit(solution)/shard_map/dot_general | solution.py:131
  414.6 2.1 copy.193
  416.7 40.9 %all_to_all.84 = bf16[8,768,256]{2,1,0:T(8,128)(2,1)S(1)} all-to-all(bf16[8,768,256]{2,1,0:T(8,128)(2,1)S(1)} %bitcast.166), channel_id=1, replica_groups=mesh['fs'=16,'tp'=8] {'tp'}, dimensions={0} | all-to-all | bytes 6291456 | tf_op jit(solution)/shard_map/all_to_all | solution.py:35
  (137 shorter events, 28.2 us)
Async XLA Ops:
  6.5 16.4 %copy-start = (bf16[768,256]{1,0:T(8,128)(2,1)S(1)}, bf16[768,256]{1,0:T(8,128)(2,1)}, u32[]{:S(2)}) copy-start(bf16[768,256]{1,0:T(8,128)(2,1)} %param.24) | copy-start | bytes 1179652
  6.5 16.4 %copy-start.20 = (f32[256]{0:T(256)S(1)}, f32[256]{0:T(256)}, u32[]{:S(2)}) copy-start(f32[256]{0:T(256)} %param.25) | copy-start | bytes 3076
  8.4 10.5 %all-to-all-start = ((f32[8,1,768]{2,1,0:T(1,128)}), f32[8,1,768]{2,1,0:T(1,128)S(1)}, u32[]{:S(2)}, u32[]{:S(2)}) async-start(f32[8,1,768]{2,1,0:T(1,128)} %broadcast_in_dim.23), calls=%async_computation | async-start | bytes 49152 | tf_op jit(solution)/shard_map/all_to_all | solution.py:20
  14.2 80.6 %all-gather.3.cloned.1.call-start = ((), (), s32[]{:S(2)}) async-start(), calls=%async_computation.11 | async-start | bytes 3342336 | tf_op jit(solution)/shard_map/all_gather | solution.py:42
  38.3 5.2 %copy-start.14 = (f32[384,128]{1,0:T(8,128)S(1)}, f32[384,128]{1,0:T(8,128)}, u32[]{:S(2)}) copy-start(f32[384,128]{1,0:T(8,128)} %param.28) | copy-start | bytes 589828
  38.3 42.7 %all-to-all-start.1 = ((bf16[768,8,256]{2,0,1:T(8,128)(2,1)}), bf16[768,8,256]{2,0,1:T(8,128)(2,1)}, u32[]{:S(2)}, u32[]{:S(2)}) async-start(bf16[768,8,256]{2,0,1:T(8,128)(2,1)} %copy.150), calls=%async_computation.1 | async-start | bytes 6291456 | tf_op jit(solution)/shard_map/all_to_all | solution.py:15
  82.3 30.0 %all-to-all-start.2 = ((bf16[16,384,128]{1,2,0:T(8,128)(2,1)}), bf16[16,384,128]{1,2,0:T(8,128)(2,1)S(1)}, u32[]{:S(2)}, u32[]{:S(2)}) async-start(bf16[16,384,128]{1,2,0:T(8,128)(2,1)} %broadcast_in_dim.24), calls=%async_computation.2 | async-start | bytes 3145728 | tf_op jit(solution)/shard_map/all_to_all | solution.py:20
  90.1 4.7 %copy-start.25 = (f32[384]{0:T(512)S(1)}, f32[384]{0:T(512)}, u32[]{:S(2)}) copy-start(f32[384]{0:T(512)} %param.29) | copy-start | bytes 4612
  94.8 17.5 %copy-start.26 = (f32[384]{0:T(512)S(1)}, f32[384]{0:T(512)}, u32[]{:S(2)}) copy-start(f32[384]{0:T(512)} %param.30) | copy-start | bytes 4612
  112.3 8.2 %copy-start.8 = (bf16[16,384,128]{1,2,0:T(8,128)(2,1)}, bf16[16,384,128]{1,2,0:T(8,128)(2,1)S(1)}, u32[]{:S(2)}) copy-start(bf16[16,384,128]{1,2,0:T(8,128)(2,1)S(1)} %all-to-all-done.2) | copy-start | bytes 4718596
  124.3 7.6 %copy-start.15 = (f32[128,256]{1,0:T(8,128)S(1)}, f32[128,256]{1,0:T(8,128)}, u32[]{:S(2)}) copy-start(f32[128,256]{1,0:T(8,128)} %param.33) | copy-start | bytes 393220
  124.3 7.7 %copy-start.16 = (f32[128,256]{1,0:T(8,128)S(1)}, f32[128,256]{1,0:T(8,128)}, u32[]{:S(2)}) copy-start(f32[128,256]{1,0:T(8,128)} %param.34) | copy-start | bytes 393220
  124.3 7.7 %copy-start.17 = (f32[128,256]{1,0:T(8,128)S(1)}, f32[128,256]{1,0:T(8,128)}, u32[]{:S(2)}) copy-start(f32[128,256]{1,0:T(8,128)} %param.35) | copy-start | bytes 393220
  124.3 7.7 %copy-start.18 = (f32[128,256]{1,0:T(8,128)S(1)}, f32[128,256]{1,0:T(8,128)}, u32[]{:S(2)}) copy-start(f32[128,256]{1,0:T(8,128)} %param.36) | copy-start | bytes 393220
  124.3 8.5 %copy-start.23 = (f32[256]{0:T(256)S(1)}, f32[256]{0:T(256)}, u32[]{:S(2)}) copy-start(f32[256]{0:T(256)} %param.31) | copy-start | bytes 3076
  124.3 45.2 %all-to-all-start.3 = ((bf16[8,768,256]{2,1,0:T(8,128)(2,1)}), bf16[8,768,256]{2,1,0:T(8,128)(2,1)}, u32[]{:S(2)}, u32[]{:S(2)}) async-start(bf16[8,768,256]{2,1,0:T(8,128)(2,1)} %bitcast.160), calls=%async_computation.3 | async-start | bytes 6291456 | tf_op jit(solution)/shard_map/all_to_all | solution.py:35
  131.9 115.4 %all-gather.5.cloned.1.call-start = ((), (), s32[]{:S(2)}) async-start(), calls=%async_computation.12 | async-start | bytes 4456448 | tf_op jit(solution)/shard_map/all_gather | solution.py:42
  132.0 48.3 %copy-start.21 = (f32[256]{0:T(256)S(1)}, f32[256]{0:T(256)}, u32[]{:S(2)}) copy-start(f32[256]{0:T(256)} %param.32) | copy-start | bytes 3076
  194.3 6.2 %copy-start.19 = (f32[256,128]{1,0:T(8,128)S(1)}, f32[256,128]{1,0:T(8,128)}, u32[]{:S(2)}) copy-start(f32[256,128]{1,0:T(8,128)} %param.43) | copy-start | bytes 393220
  194.3 42.7 %all-to-all-start.5 = ((bf16[768,8,256]{2,0,1:T(8,128)(2,1)}), bf16[768,8,256]{2,0,1:T(8,128)(2,1)}, u32[]{:S(2)}, u32[]{:S(2)}) async-start(bf16[768,8,256]{2,0,1:T(8,128)(2,1)} %copy.156), calls=%async_computation.5 | async-start | bytes 6291456 | tf_op jit(solution)/shard_map/all_to_all | solution.py:15
  238.1 47.8 %all-to-all-start.6 = ((bf16[16,256,128]{1,2,0:T(8,128)(2,1)}), bf16[16,256,128]{1,2,0:T(8,128)(2,1)}, u32[]{:S(2)}, u32[]{:S(2)}) async-start(bf16[16,256,128]{1,2,0:T(8,128)(2,1)} %broadcast_in_dim.31), calls=%async_computation.6 | async-start | bytes 2097152 | tf_op jit(solution)/shard_map/all_to_all | solution.py:20
  242.6 4.7 %copy-start.27 = (f32[256]{0:T(256)S(1)}, f32[256]{0:T(256)}, u32[]{:S(2)}) copy-start(f32[256]{0:T(256)} %param.38) | copy-start | bytes 3076
  252.2 2.2 copy-start.1
  252.2 2.2 copy-start.28
  256.6 0.9 copy-start.2
  258.2 2.2 copy-start.13
  258.4 3.1 copy-start.3
  258.5 4.3 copy-start.29
  262.8 3.4 copy-start.4
  262.8 3.4 copy-start.5
  262.8 3.5 copy-start.6
  262.8 3.5 copy-start.7
  262.8 3.5 copy-start.10
  262.8 3.5 copy-start.11
  262.8 3.5 copy-start.12
  329.2 0.7 copy-start.24
  329.2 9.0 %copy-start.22 = (f32[256]{0:T(256)S(1)}, f32[256]{0:T(256)}, u32[]{:S(2)}) copy-start(f32[256]{0:T(256)} %param.45) | copy-start | bytes 3076
  402.8 4.3 copy-start.9
Sparse Core Ops, SparseCore 0:
  17.1 49.5 all-gather.2
  134.9 48.3 all-gather.4
